TPU v7x, 32 devices: a whole 2x2x4 slice. The times are simulated.
32 devices in a mesh: tp: 8 (over z, y), dp: 4 (over x, core).
Axes of the slice: x: 2, y: 2, z: 4, core: 2. Of those that a mesh axis runs over, the one named last changes fastest.
Arguments:
- stream: bfloat16 [256, 2048], P('tp', 'dp'), may hold values from -12 to 12
- norm_gain: float32 [2, 2048], P(None, 'dp'), may hold values from 0.1 to 1.9
- w_input: bfloat16 [2, 2048, 2048], P(None, 'dp', 'tp'), may hold values from -0.125 to 0.125
- lam_re: float32 [2, 128, 64], P(None, 'tp'), may hold values from -1 to -0.05
- lam_im: float32 [2, 128, 64], P(None, 'tp'), may hold values from 0 to 6
- log_dt: float32 [2, 128], P(None, 'tp'), may hold values from -3 to 0
- b_re: float32 [2, 128, 64, 16], P(None, 'tp'), may hold values from -1 to 1
- b_im: float32 [2, 128, 64, 16], P(None, 'tp'), may hold values from -1 to 1
- readout_real: float32 [2, 128, 16, 64], P(None, 'tp'), may hold values from -0.5 to 0.5
- readout_imaginary: float32 [2, 128, 16, 64], P(None, 'tp'), may hold values from -0.5 to 0.5
- d_skip: float32 [2, 2048], P(None, 'tp'), may hold values from -4 to 4
- w_val: bfloat16 [2, 2048, 2048], P(None, 'tp', 'dp'), may hold values from -0.375 to 0.375
- w_gate: bfloat16 [2, 2048, 2048], P(None, 'tp', 'dp'), may hold values from -0.375 to 0.375
- state: float32 [2, 256, 128, 128], P(None, 'dp', 'tp'), may hold values from -6 to 6
Outputs:
- stream_out: bfloat16 [256, 2048], P('tp', 'dp')
- states_out: float32 [2, 256, 128, 128], P(None, 'dp', 'tp')
All inputs are finite; a program needn't handle non-finite values.
Results may differ from a plain program's by a relative error of at most 0.0064.
Values may be sent and summed in bfloat16 or wider, within the bound.
A program may use at most 64 MiB of HBM per device.

v0:
```python
import jax
import jax.numpy as jnp
from jax import lax
from jax.sharding import PartitionSpec as P

D = 2048
LAYERS = 2
eps = 1e-06


def advance(
    inputs, old_state, lam_re, lam_im, log_dt, b_re, b_im, readout_real, readout_imaginary, d_skip
):
    upper_bound = lax.Precision.HIGHEST
    count_rows, groups, doubled = old_state.shape
    half_state = doubled // 2
    chans = b_re.shape[-1]
    step_size = jnp.exp(log_dt)[:, None]
    decay = jnp.exp(lam_re * step_size)
    angle = lam_im * step_size
    keep_re = decay * jnp.cos(angle)
    keep_im = decay * jnp.sin(angle)
    denom = lam_re * lam_re + lam_im * lam_im
    ratio_re = ((keep_re - 1.0) * lam_re + keep_im * lam_im) / denom
    ratio_im = (keep_im * lam_re - (keep_re - 1.0) * lam_im) / denom
    drive_re = ratio_re[..., None] * b_re - ratio_im[..., None] * b_im
    drive_im = ratio_re[..., None] * b_im + ratio_im[..., None] * b_re
    grouped = inputs.reshape(count_rows, groups, chans)
    push_re = jnp.einsum("gpc,rgc->rgp", drive_re, grouped, precision=upper_bound)
    push_im = jnp.einsum("gpc,rgc->rgp", drive_im, grouped, precision=upper_bound)
    old_re = old_state[..., :half_state]
    old_im = old_state[..., half_state:]
    updated_real = keep_re * old_re - keep_im * old_im + push_re
    updated_imaginary = keep_re * old_im + keep_im * old_re + push_im
    readout_output = jnp.einsum(
        "aot,mat->mao", readout_real, updated_real, precision=upper_bound
    ) - jnp.einsum("aot,mat->mao", readout_imaginary, updated_imaginary, precision=upper_bound)
    pre_act = readout_output.reshape(count_rows, groups * chans) + d_skip * inputs
    return (pre_act, jnp.concatenate([updated_real, updated_imaginary], axis=-1))


def half_output(mixed_all, val_part, gate_part):
    return jnp.concatenate(
        [
            jnp.dot(mixed_all, val_part, preferred_element_type=jnp.float32),
            jnp.dot(mixed_all, gate_part, preferred_element_type=jnp.float32),
        ],
        axis=1,
    )


def per_device(
    stream,
    norm_gain,
    w_input,
    lam_re,
    lam_im,
    log_dt,
    b_re,
    b_im,
    readout_real,
    readout_imaginary,
    d_skip,
    w_val,
    w_gate,
    state,
):
    collected = []
    for layer_no in range(LAYERS):
        gathered = lax.all_gather(stream, "tp", axis=0, tiled=True)
        widened = gathered.astype(jnp.float32)
        normed = (widened * norm_gain[layer_no]).astype(jnp.bfloat16)
        square_part = jnp.sum(widened * widened, axis=1)
        weight_in = w_input[layer_no]
        partial_value = jnp.dot(normed, weight_in, preferred_element_type=jnp.float32)
        summed, square_total = (
            lax.psum_scatter(partial_value, "dp", scatter_dimension=0, tiled=True),
            lax.psum_scatter(square_part, "dp", scatter_dimension=0, tiled=True),
        )
        inputs = lax.rsqrt(square_total / D + eps)[:, None] * summed
        pre_act, new_state = advance(
            inputs,
            state[layer_no],
            lam_re[layer_no],
            lam_im[layer_no],
            log_dt[layer_no],
            b_re[layer_no],
            b_im[layer_no],
            readout_real[layer_no],
            readout_imaginary[layer_no],
            d_skip[layer_no],
        )
        mixed = jax.nn.gelu(pre_act).astype(jnp.bfloat16)
        mixed_all = lax.all_gather(mixed, "dp", axis=0, tiled=True)
        columns = w_val.shape[2]
        combined = lax.psum_scatter(
            half_output(mixed_all, w_val[layer_no], w_gate[layer_no]),
            "tp",
            scatter_dimension=0,
            tiled=True,
        )
        value = combined[:, :columns]
        gate = combined[:, columns:]
        stream = (stream.astype(jnp.float32) + value * jax.nn.sigmoid(gate)).astype(jnp.bfloat16)
        collected.append(new_state)
    return (stream, jnp.stack(collected))


def solution(mesh):
    return jax.shard_map(
        per_device,
        mesh=mesh,
        in_specs=(
            P("tp", "dp"),
            P(None, "dp"),
            P(None, "dp", "tp"),
            P(None, "tp", None),
            P(None, "tp", None),
            P(None, "tp"),
            P(None, "tp", None, None),
            P(None, "tp", None, None),
            P(None, "tp", None, None),
            P(None, "tp", None, None),
            P(None, "tp"),
            P(None, "tp", "dp"),
            P(None, "tp", "dp"),
            P(None, "dp", "tp", None),
        ),
        out_specs=(P("tp", "dp"), P(None, "dp", "tp", None)),
        check_vma=False,
    )
```

profile of v0, /device:TPU:0, one launch (start us, length us, event | category | flops | bytes accessed | tf_op | source)
XLA Modules:
  0.0 278.8 jit_solution(17151186009216203104)
XLA Ops:
  8.0 32.8 %all_gather.12 = bf16[256,512]{1,0:T(8,128)(2,1)S(1)} all-gather(bf16[32,512]{1,0:T(8,128)(2,1)} %param.14), channel_id=1, replica_groups=mesh['tp'=8,'dp'=4] {'tp'}, dimensions={0}, use_global_device_ids=true | all-gather | bytes 294912 | tf_op jit(solution)/shard_map/all_gather | solution.py:70
  40.8 1.9 fusion.10
  44.4 5.6 %all-reduce = f32[256]{0:T(256)S(1)} all-reduce(f32[256]{0:T(256)S(1)} %fusion.4), channel_id=2, replica_groups=mesh['tp'=8,'dp'=4] {'dp'}, use_global_device_ids=true, to_apply=%region_1.0.clone | all-reduce | flops 256 | bytes 2048
  52.5 11.4 %reduce-scatter.5.cloned.1.call-done = f32[64,256]{1,0:T(8,128)} async-done(((f32[256,256]{1,0:T(8,128)}), f32[64,256]{1,0:T(8,128)}) %reduce-scatter.5.cloned.1.call-update) | async-done | bytes 65552 | tf_op jit(solution)/shard_map/reduce_scatter | solution.py:77
  64.9 1.0 fusion.3
  65.9 1.0 fusion.2
  67.0 0.9 fusion.38
  68.0 0.9 convolution_subtract_fusion.1
  69.8 5.5 %all_gather.13 = bf16[256,256]{1,0:T(8,128)(2,1)S(1)} all-gather(bf16[64,256]{1,0:T(8,128)(2,1)S(1)} %fusion.63), channel_id=1, replica_groups=mesh['tp'=8,'dp'=4] {'dp'}, dimensions={0}, use_global_device_ids=true | all-gather | bytes 163840 | tf_op jit(solution)/shard_map/all_gather | solution.py:94
  75.9 1.1 pad_maximum_fusion
  77.0 64.3 %reduce-scatter.7.cloned.1.call-done = f32[32,1024]{1,0:T(8,128)} async-done(((f32[256,1024]{1,0:T(8,128)}), f32[32,1024]{1,0:T(8,128)}) %reduce-scatter.7.cloned.1.call-update) | async-done | bytes 131088 | tf_op jit(solution)/shard_map/reduce_scatter | solution.py:96
  142.3 30.9 %all_gather.14 = bf16[256,512]{1,0:T(8,128)(2,1)S(1)} all-gather(bf16[32,512]{1,0:T(8,128)(2,1)S(1)} %fusion.90), channel_id=1, replica_groups=mesh['tp'=8,'dp'=4] {'tp'}, dimensions={0}, use_global_device_ids=true | all-gather | bytes 294912 | tf_op jit(solution)/shard_map/all_gather | solution.py:70
  173.1 0.9 fusion.8
  174.3 5.7 %all-reduce.1 = f32[256]{0:T(256)S(1)} all-reduce(f32[256]{0:T(256)S(1)} %fusion.6), channel_id=5, replica_groups=mesh['tp'=8,'dp'=4] {'dp'}, use_global_device_ids=true, to_apply=%region_5.0.clone | all-reduce | flops 256 | bytes 2048
  180.0 13.2 %reduce-scatter.9.cloned.1.call-done = f32[64,256]{1,0:T(8,128)} async-done(((f32[256,256]{1,0:T(8,128)}), f32[64,256]{1,0:T(8,128)}) %reduce-scatter.9.cloned.1.call-update) | async-done | bytes 65552 | tf_op jit(solution)/shard_map/reduce_scatter | solution.py:77
  194.3 1.0 fusion
  195.3 1.0 fusion.1
  196.4 0.9 fusion.31
  197.3 0.9 convolution_subtract_fusion
  199.2 5.5 %all_gather.15 = bf16[256,256]{1,0:T(8,128)(2,1)S(1)} all-gather(bf16[64,256]{1,0:T(8,128)(2,1)S(1)} %fusion.71), channel_id=1, replica_groups=mesh['tp'=8,'dp'=4] {'dp'}, dimensions={0}, use_global_device_ids=true | all-gather | bytes 163840 | tf_op jit(solution)/shard_map/all_gather | solution.py:94
  205.2 1.1 pad_maximum_fusion.1
  206.9 1.6 copy.38
  208.5 62.3 %reduce-scatter.11.cloned.1.call-done = f32[32,1024]{1,0:T(8,128)} async-done(((f32[256,1024]{1,0:T(8,128)}), f32[32,1024]{1,0:T(8,128)}) %reduce-scatter.11.cloned.1.call-update) | async-done | bytes 131088 | tf_op jit(solution)/shard_map/reduce_scatter | solution.py:96
  270.7 1.5 fusion.91
  (76 shorter events, 10.9 us)
Async XLA Ops:
  7.2 44.9 %copy-start.2 = (f32[2,64,16,128]{3,2,1,0:T(8,128)S(1)}, f32[2,64,16,128]{3,2,1,0:T(8,128)}, u32[]{:S(2)}) copy-start(f32[2,64,16,128]{3,2,1,0:T(8,128)} %param.27) | copy-start | bytes 3145732
  7.2 56.7 %reduce-scatter.5.cloned.1.call-start = ((), (), s32[]{:S(2)}) async-start(), calls=%async_computation.4 | async-start | bytes 327680 | tf_op jit(solution)/shard_map/reduce_scatter | solution.py:77
  42.7 0.8 copy-start.15
  42.7 0.8 copy-start.16
  42.7 98.7 %reduce-scatter.7.cloned.1.call-start = ((), (), s32[]{:S(2)}) async-start(), calls=%async_computation.5 | async-start | bytes 1179648 | tf_op jit(solution)/shard_map/reduce_scatter | solution.py:96
  42.7 0.7 copy-start.18
  43.7 0.7 copy-start.17
  50.1 0.7 copy-start.19
  52.1 12.7 %copy-start.1 = (f32[2,16,64,16]{2,3,1,0:T(8,128)S(1)}, f32[2,16,64,16]{2,3,1,0:T(8,128)}, u32[]{:S(2)}) copy-start(f32[2,16,64,16]{2,3,1,0:T(8,128)} %param.20) | copy-start | bytes 393220
  52.5 12.4 %copy-start = (f32[2,16,64,16]{2,3,1,0:T(8,128)S(1)}, f32[2,16,64,16]{2,3,1,0:T(8,128)}, u32[]{:S(2)}) copy-start(f32[2,16,64,16]{2,3,1,0:T(8,128)} %param.21) | copy-start | bytes 393220
  65.9 1.1 copy-start.12
  67.0 1.0 copy-start.8
  68.0 7.5 %copy-start.4 = (bf16[2,256,512]{2,1,0:T(8,128)(2,1)S(1)}, bf16[2,256,512]{2,1,0:T(8,128)(2,1)}, u32[]{:S(2)}) copy-start(bf16[2,256,512]{2,1,0:T(8,128)(2,1)} %param.26) | copy-start | bytes 1572868
  68.9 0.9 copy-start.10
  69.8 5.8 %copy-start.6 = (bf16[2,256,512]{2,1,0:T(8,128)(2,1)S(1)}, bf16[2,256,512]{2,1,0:T(8,128)(2,1)}, u32[]{:S(2)}) copy-start(bf16[2,256,512]{2,1,0:T(8,128)(2,1)} %param.25) | copy-start | bytes 1572868
  76.9 64.4 %copy-start.14 = (bf16[32,512]{1,0:T(8,128)(2,1)S(1)}, bf16[32,512]{1,0:T(8,128)(2,1)}, u32[]{:S(2)}) copy-start(bf16[32,512]{1,0:T(8,128)(2,1)} %param.14) | copy-start | bytes 98308
  76.9 96.2 %copy-start.3 = (bf16[2,512,256]{2,1,0:T(8,128)(2,1)S(1)}, bf16[2,512,256]{2,1,0:T(8,128)(2,1)}, u32[]{:S(2)}) copy-start(bf16[2,512,256]{2,1,0:T(8,128)(2,1)} %param.16) | copy-start | bytes 1572868
  77.0 116.3 %reduce-scatter.9.cloned.1.call-start = ((), (), s32[]{:S(2)}) async-start(), calls=%async_computation.6 | async-start | bytes 327680 | tf_op jit(solution)/shard_map/reduce_scatter | solution.py:77
  174.1 96.6 %reduce-scatter.11.cloned.1.call-start = ((), (), s32[]{:S(2)}) async-start(), calls=%async_computation.7 | async-start | bytes 1179648 | tf_op jit(solution)/shard_map/reduce_scatter | solution.py:96
  195.3 1.1 copy-start.13
  196.4 1.0 copy-start.9
  197.3 7.4 %copy-start.5 = (bf16[2,256,512]{2,1,0:T(8,128)(2,1)S(1)}, bf16[2,256,512]{2,1,0:T(8,128)(2,1)}, u32[]{:S(2)}) copy-start(bf16[2,256,512]{2,1,0:T(8,128)(2,1)} %param.26) | copy-start | bytes 1572868
  198.3 0.9 copy-start.11
  199.2 5.8 %copy-start.7 = (bf16[2,256,512]{2,1,0:T(8,128)(2,1)S(1)}, bf16[2,256,512]{2,1,0:T(8,128)(2,1)}, u32[]{:S(2)}) copy-start(bf16[2,256,512]{2,1,0:T(8,128)(2,1)} %param.25) | copy-start | bytes 1572868
Sparse Core Ops, SparseCore 0:
  42.8 21.0 reduce-scatter.4
  77.1 64.2 reduce-scatter.6
  174.2 18.9 reduce-scatter.8
  206.5 64.2 reduce-scatter.10
where the time goes:
time: 279 us
  waiting for transfers between devices  151 us (54%)
  blocking collectives  86 us (31%)
  between operations  14.7 us (5%)
  matrix products  11.6 us (4%)
  other arithmetic  7.83 us (3%)
  local copies, waits for them, and re-layouts  7.2 us (3%)
    reduce_scatter x2, waiting for transfers between devices, per_device(): lax.psum_scatter(half_output(mixed_all, w_val[layer_no], w_gate[layer_no]...  127 us
    all_gather x2, blocking collectives, per_device(): gathered = lax.all_gather(stream, 'tp', axis=0, tiled=True)  63.6 us
    reduce_scatter x2, waiting for transfers between devices, per_device(): lax.psum_scatter(partial_value, 'dp', scatter_dimension=0, tiled=True)  24.6 us
    unnamed x2, blocking collectives  11.3 us
    all_gather x2, blocking collectives, per_device(): mixed_all = lax.all_gather(mixed, 'dp', axis=0, tiled=True)  11.1 us
    unnamed x42, local copies, waits for them, and re-layouts  5.66 us
  transfers between devices with their start and end apart: 4, of which 4 were waited for; matrix products, arithmetic and copies ran while one was open for 1% of the time, Pallas kernels for 0%

commit v1 on v0

--- a/solution.py
+++ b/solution.py
@@ -6,6 +6,27 @@
 D = 2048
 LAYERS = 2
 eps = 1e-06
+
+
+def laid_out(tiles, dim):
+    tiles = jnp.moveaxis(tiles, 0, dim)
+    shape = tiles.shape
+    return tiles.reshape(*shape[:dim], shape[dim] * shape[dim + 1], *shape[dim + 2 :])
+
+
+def doubled_2(shard, axis):
+    devices, place = (lax.axis_size(axis), lax.axis_index(axis))
+    blocks, bit = (shard[None], 1)
+    while bit < devices:
+        other = lax.ppermute(blocks, axis, [(i, i ^ bit) for i in range(devices)])
+        low = place & bit == 0
+        blocks = jnp.concatenate([jnp.where(low, blocks, other), jnp.where(low, other, blocks)])
+        bit *= 2
+    return blocks
+
+
+def collect(array, axis, dim):
+    return laid_out(doubled_2(array, axis), dim)
 
 
 def advance(
@@ -67,7 +88,7 @@
 ):
     collected = []
     for layer_no in range(LAYERS):
-        gathered = lax.all_gather(stream, "tp", axis=0, tiled=True)
+        gathered = collect(stream, "tp", 0)
         widened = gathered.astype(jnp.float32)
         normed = (widened * norm_gain[layer_no]).astype(jnp.bfloat16)
         square_part = jnp.sum(widened * widened, axis=1)

time: 279 us -> 249 us (0.89)
  blocking collectives: 86 us -> 22.4 us
  waiting for transfers between devices: 151 us -> 173 us
  starting transfers between devices: 0.16 us -> 11.8 us
    all_gather x2 -> x0, blocking collectives: 63.6 us -> none  [per_device(): gathered = lax.all_gather(stream, 'tp', axis=0, tiled=True)]
    ppermute x0 -> x6, waiting for transfers between devices: none -> 19.1 us  [doubled_2(): other = lax.ppermute(blocks, axis, [(i, i ^ bit) for i in range(devices)])]
    ppermute x0 -> x6, starting transfers between devices: none -> 11.6 us  [doubled_2(): other = lax.ppermute(blocks, axis, [(i, i ^ bit) for i in range(devices)])]
    reduce_scatter x2, waiting for transfers between devices: 24.6 us -> 27.5 us  [per_device(): lax.psum_scatter(partial_value, 'dp', scatter_dimension=0, tiled=True)]
    unnamed x42 -> x44, local copies, waits for them, and re-layouts: 5.66 us -> 5.05 us
  transfers between devices with their start and end apart: 4 -> 10, of which waited for: 4 -> 10; matrix products, arithmetic and copies ran while one was open for 1% -> 2% of each run, Pallas kernels for 0% -> 0%
where the time goes in v1:
time: 249 us; the launch traced here: 248 us
  waiting for transfers between devices  173 us (69%)
  blocking collectives  22.4 us (9%)
  between operations  14.8 us (6%)
  starting transfers between devices  11.8 us (5%)
  matrix products  10.6 us (4%)
  other arithmetic  7.98 us (3%)
  local copies, waits for them, and re-layouts  7.18 us (3%)
    reduce_scatter x2, waiting for transfers between devices, per_device(): lax.psum_scatter(half_output(mixed_all, w_val[layer_no], w_gate[layer_no]...  127 us
    reduce_scatter x2, waiting for transfers between devices, per_device(): lax.psum_scatter(partial_value, 'dp', scatter_dimension=0, tiled=True)  27.5 us
    ppermute x6, waiting for transfers between devices, doubled_2(): other = lax.ppermute(blocks, axis, [(i, i ^ bit) for i in range(devices)])  19.1 us
    ppermute x6, starting transfers between devices, doubled_2(): other = lax.ppermute(blocks, axis, [(i, i ^ bit) for i in range(devices)])  11.6 us
    unnamed x2, blocking collectives  11.3 us
    all_gather x2, blocking collectives, per_device(): mixed_all = lax.all_gather(mixed, 'dp', axis=0, tiled=True)  11.1 us
    unnamed x44, local copies, waits for them, and re-layouts  5.05 us
  transfers between devices with their start and end apart: 10, of which 10 were waited for; matrix products, arithmetic and copies ran while one was open for 2% of the time, Pallas kernels for 0%

profile of v1, /device:TPU:0, one launch (start us, length us, event | category | flops | bytes accessed | tf_op | source)
XLA Modules:
  0.0 248.1 jit_solution(7049027057876351220)
XLA Ops:
  7.2 3.1 %collective-permute-start = (bf16[1,32,512]{2,1,0:T(8,128)(2,1)}, bf16[1,32,512]{2,1,0:T(8,128)(2,1)S(1)}, u32[]{:S(2)}, u32[]{:S(2)}) collective-permute-start(bf16[1,32,512]{2,1,0:T(8,128)(2,1)} %bitcast.262), channel_id=1, source_target_pairs={{0,4},{4,0},{8,12},{12,8},{16,20},{20,16},{24,28},{28,24},{1,5},{5... | collective-permute-start | bytes 98312 | tf_op jit(solution)/shard_map/ppermute | solution.py:21
  10.3 1.3 fusion.104
  12.4 2.1 collective-permute-start.1
  16.9 3.1 %collective-permute-start.2 = (bf16[4,32,512]{2,1,0:T(8,128)(2,1)S(1)}, bf16[4,32,512]{2,1,0:T(8,128)(2,1)S(1)}, u32[]{:S(2)}, u32[]{:S(2)}) collective-permute-start(bf16[4,32,512]{2,1,0:T(8,128)(2,1)S(1)} %pad_maximum_fusion.5), channel_id=1, source_target_pairs={{0,16},{4,20},{8,24},{12,28},{16,0},{20,4},{24,8},{28,12},{1,17},{... | collective-permute-start | bytes 393224 | tf_op jit(solution)/shard_map/ppermute | solution.py:21
  20.0 4.7 %collective-permute-done.2 = bf16[4,32,512]{2,1,0:T(8,128)(2,1)S(1)} collective-permute-done((bf16[4,32,512]{2,1,0:T(8,128)(2,1)S(1)}, bf16[4,32,512]{2,1,0:T(8,128)(2,1)S(1)}, u32[]{:S(2)}, u32[]{:S(2)}) %collective-permute-start.2) | collective-permute-done | bytes 131104 | tf_op jit(solution)/shard_map/ppermute | solution.py:21
  26.9 5.6 %all-reduce = f32[256]{0:T(256)S(1)} all-reduce(f32[256]{0:T(256)S(1)} %reduce_sum.23), channel_id=2, replica_groups=mesh['tp'=8,'dp'=4] {'dp'}, use_global_device_ids=true, to_apply=%region_1.2.clone | all-reduce | flops 256 | bytes 2048
  32.6 14.6 %reduce-scatter.5.cloned.1.call-done = f32[64,256]{1,0:T(8,128)} async-done(((f32[256,256]{1,0:T(8,128)}), f32[64,256]{1,0:T(8,128)}) %reduce-scatter.5.cloned.1.call-update) | async-done | bytes 65552 | tf_op jit(solution)/shard_map/reduce_scatter | solution.py:98
  49.2 1.0 fusion.2
  53.1 5.5 %all_gather.6 = bf16[256,256]{1,0:T(8,128)(2,1)S(1)} all-gather(bf16[64,256]{1,0:T(8,128)(2,1)S(1)} %fusion.59), channel_id=1, replica_groups=mesh['tp'=8,'dp'=4] {'dp'}, dimensions={0}, use_global_device_ids=true | all-gather | bytes 163840 | tf_op jit(solution)/shard_map/all_gather | solution.py:115
  59.1 1.1 pad_maximum_fusion
  60.3 64.3 %reduce-scatter.7.cloned.1.call-done = f32[32,1024]{1,0:T(8,128)} async-done(((f32[256,1024]{1,0:T(8,128)}), f32[32,1024]{1,0:T(8,128)}) %reduce-scatter.7.cloned.1.call-update) | async-done | bytes 131088 | tf_op jit(solution)/shard_map/reduce_scatter | solution.py:117
  125.5 1.2 collective-permute-start.3
  126.7 2.8 %collective-permute-done.3 = bf16[1,32,512]{2,1,0:T(8,128)(2,1)S(1)} collective-permute-done((bf16[1,32,512]{2,1,0:T(8,128)(2,1)S(1)}, bf16[1,32,512]{2,1,0:T(8,128)(2,1)S(1)}, u32[]{:S(2)}, u32[]{:S(2)}) %collective-permute-start.3) | collective-permute-done | bytes 32800 | tf_op jit(solution)/shard_map/ppermute | solution.py:21
  129.5 1.4 collective-permute-start.4
  130.9 4.3 %collective-permute-done.4 = bf16[2,32,512]{2,1,0:T(8,128)(2,1)S(1)} collective-permute-done((bf16[2,32,512]{2,1,0:T(8,128)(2,1)S(1)}, bf16[2,32,512]{2,1,0:T(8,128)(2,1)S(1)}, u32[]{:S(2)}, u32[]{:S(2)}) %collective-permute-start.4) | collective-permute-done | bytes 65568 | tf_op jit(solution)/shard_map/ppermute | solution.py:21
  136.1 6.5 %collective-permute-done.5 = bf16[4,32,512]{2,1,0:T(8,128)(2,1)S(1)} collective-permute-done((bf16[4,32,512]{2,1,0:T(8,128)(2,1)S(1)}, bf16[4,32,512]{2,1,0:T(8,128)(2,1)S(1)}, u32[]{:S(2)}, u32[]{:S(2)}) %collective-permute-start.5) | collective-permute-done | bytes 131104 | tf_op jit(solution)/shard_map/ppermute | solution.py:21
  143.9 5.6 %all-reduce.1 = f32[256]{0:T(256)S(1)} all-reduce(f32[256]{0:T(256)S(1)} %reduce_sum.25), channel_id=5, replica_groups=mesh['tp'=8,'dp'=4] {'dp'}, use_global_device_ids=true, to_apply=%region_5.6.clone | all-reduce | flops 256 | bytes 2048
  149.6 13.0 %reduce-scatter.9.cloned.1.call-done = f32[64,256]{1,0:T(8,128)} async-done(((f32[256,256]{1,0:T(8,128)}), f32[64,256]{1,0:T(8,128)}) %reduce-scatter.9.cloned.1.call-update) | async-done | bytes 65552 | tf_op jit(solution)/shard_map/reduce_scatter | solution.py:98
  163.6 1.0 fusion
  168.5 5.5 %all_gather.7 = bf16[256,256]{1,0:T(8,128)(2,1)S(1)} all-gather(bf16[64,256]{1,0:T(8,128)(2,1)S(1)} %fusion.67), channel_id=1, replica_groups=mesh['tp'=8,'dp'=4] {'dp'}, dimensions={0}, use_global_device_ids=true | all-gather | bytes 163840 | tf_op jit(solution)/shard_map/all_gather | solution.py:115
  174.6 1.1 pad_maximum_fusion.1
  176.2 1.6 copy.38
  177.7 62.3 %reduce-scatter.11.cloned.1.call-done = f32[32,1024]{1,0:T(8,128)} async-done(((f32[256,1024]{1,0:T(8,128)}), f32[32,1024]{1,0:T(8,128)}) %reduce-scatter.11.cloned.1.call-update) | async-done | bytes 131088 | tf_op jit(solution)/shard_map/reduce_scatter | solution.py:117
  240.0 1.5 fusion.87
  (100 shorter events, 19.0 us)
Async XLA Ops:
  7.2 3.1 %copy-start.19 = (f32[2,16]{1,0:T(2,128)S(1)}, f32[2,16]{1,0:T(2,128)}, u32[]{:S(2)}) copy-start(f32[2,16]{1,0:T(2,128)} %param.19) | copy-start | bytes 388
  7.2 40.0 %reduce-scatter.5.cloned.1.call-start = ((), (), s32[]{:S(2)}) async-start(), calls=%async_computation.4 | async-start | bytes 327680 | tf_op jit(solution)/shard_map/reduce_scatter | solution.py:98
  7.2 5.2 %collective-permute-start = (bf16[1,32,512]{2,1,0:T(8,128)(2,1)}, bf16[1,32,512]{2,1,0:T(8,128)(2,1)S(1)}, u32[]{:S(2)}, u32[]{:S(2)}) collective-permute-start(bf16[1,32,512]{2,1,0:T(8,128)(2,1)} %bitcast.262), channel_id=1, source_target_pairs={{0,4},{4,0},{8,12},{12,8},{16,20},{20,16},{24,28},{28,24},{1,5},{5... | collective-permute-start | bytes 98312 | tf_op jit(solution)/shard_map/ppermute | solution.py:21
  10.3 1.3 copy-start.15
  10.3 1.3 copy-start.16
  12.4 4.4 %collective-permute-start.1 = (bf16[2,32,512]{2,1,0:T(8,128)(2,1)S(1)}, bf16[2,32,512]{2,1,0:T(8,128)(2,1)S(1)}, u32[]{:S(2)}, u32[]{:S(2)}) collective-permute-start(bf16[2,32,512]{2,1,0:T(8,128)(2,1)S(1)} %pad_maximum_fusion.7), channel_id=1, source_target_pairs={{0,8},{4,12},{8,0},{12,4},{16,24},{20,28},{24,16},{28,20},{1,9},{5... | collective-permute-start | bytes 196616 | tf_op jit(solution)/shard_map/ppermute | solution.py:21
  16.8 3.1 %copy-start.17 = (f32[2,512]{1,0:T(2,128)S(1)}, f32[2,512]{1,0:T(2,128)}, u32[]{:S(2)}) copy-start(f32[2,512]{1,0:T(2,128)} %param.15) | copy-start | bytes 12292
  16.9 7.8 %collective-permute-start.2 = (bf16[4,32,512]{2,1,0:T(8,128)(2,1)S(1)}, bf16[4,32,512]{2,1,0:T(8,128)(2,1)S(1)}, u32[]{:S(2)}, u32[]{:S(2)}) collective-permute-start(bf16[4,32,512]{2,1,0:T(8,128)(2,1)S(1)} %pad_maximum_fusion.5), channel_id=1, source_target_pairs={{0,16},{4,20},{8,24},{12,28},{16,0},{20,4},{24,8},{28,12},{1,17},{... | collective-permute-start | bytes 393224 | tf_op jit(solution)/shard_map/ppermute | solution.py:21
  20.0 4.8 %copy-start.2 = (bf16[2,512,256]{2,1,0:T(8,128)(2,1)S(1)}, bf16[2,512,256]{2,1,0:T(8,128)(2,1)}, u32[]{:S(2)}) copy-start(bf16[2,512,256]{2,1,0:T(8,128)(2,1)} %param.16) | copy-start | bytes 1572868
  25.8 98.8 %reduce-scatter.7.cloned.1.call-start = ((), (), s32[]{:S(2)}) async-start(), calls=%async_computation.5 | async-start | bytes 1179648 | tf_op jit(solution)/shard_map/reduce_scatter | solution.py:117
  26.4 21.7 %copy-start.1 = (f32[2,16,64,16]{2,3,1,0:T(8,128)S(1)}, f32[2,16,64,16]{2,3,1,0:T(8,128)}, u32[]{:S(2)}) copy-start(f32[2,16,64,16]{2,3,1,0:T(8,128)} %param.20) | copy-start | bytes 393220
  26.8 21.4 %copy-start = (f32[2,16,64,16]{2,3,1,0:T(8,128)S(1)}, f32[2,16,64,16]{2,3,1,0:T(8,128)}, u32[]{:S(2)}) copy-start(f32[2,16,64,16]{2,3,1,0:T(8,128)} %param.21) | copy-start | bytes 393220
  49.2 1.1 copy-start.12
  51.2 7.5 %copy-start.4 = (bf16[2,256,512]{2,1,0:T(8,128)(2,1)S(1)}, bf16[2,256,512]{2,1,0:T(8,128)(2,1)}, u32[]{:S(2)}) copy-start(bf16[2,256,512]{2,1,0:T(8,128)(2,1)} %param.26) | copy-start | bytes 1572868
  53.1 5.8 %copy-start.6 = (bf16[2,256,512]{2,1,0:T(8,128)(2,1)S(1)}, bf16[2,256,512]{2,1,0:T(8,128)(2,1)}, u32[]{:S(2)}) copy-start(bf16[2,256,512]{2,1,0:T(8,128)(2,1)} %param.25) | copy-start | bytes 1572868
  60.2 102.3 %reduce-scatter.9.cloned.1.call-start = ((), (), s32[]{:S(2)}) async-start(), calls=%async_computation.6 | async-start | bytes 327680 | tf_op jit(solution)/shard_map/reduce_scatter | solution.py:98
  125.5 4.0 %collective-permute-start.3 = (bf16[1,32,512]{2,1,0:T(8,128)(2,1)S(1)}, bf16[1,32,512]{2,1,0:T(8,128)(2,1)S(1)}, u32[]{:S(2)}, u32[]{:S(2)}) collective-permute-start(bf16[1,32,512]{2,1,0:T(8,128)(2,1)S(1)} %bitcast.261), channel_id=1, source_target_pairs={{0,4},{4,0},{8,12},{12,8},{16,20},{20,16},{24,28},{28,24},{1,5},{5... | collective-permute-start | bytes 98312 | tf_op jit(solution)/shard_map/ppermute | solution.py:21
  129.5 5.7 %collective-permute-start.4 = (bf16[2,32,512]{2,1,0:T(8,128)(2,1)S(1)}, bf16[2,32,512]{2,1,0:T(8,128)(2,1)S(1)}, u32[]{:S(2)}, u32[]{:S(2)}) collective-permute-start(bf16[2,32,512]{2,1,0:T(8,128)(2,1)S(1)} %pad_maximum_fusion.8), channel_id=1, source_target_pairs={{0,8},{4,12},{8,0},{12,4},{16,24},{20,28},{24,16},{28,20},{1,9},{5... | collective-permute-start | bytes 196616 | tf_op jit(solution)/shard_map/ppermute | solution.py:21
  135.2 7.5 %copy-start.3 = (bf16[2,512,256]{2,1,0:T(8,128)(2,1)S(1)}, bf16[2,512,256]{2,1,0:T(8,128)(2,1)}, u32[]{:S(2)}) copy-start(bf16[2,512,256]{2,1,0:T(8,128)(2,1)} %param.16) | copy-start | bytes 1572868
  135.3 7.3 %collective-permute-start.5 = (bf16[4,32,512]{2,1,0:T(8,128)(2,1)S(1)}, bf16[4,32,512]{2,1,0:T(8,128)(2,1)S(1)}, u32[]{:S(2)}, u32[]{:S(2)}) collective-permute-start(bf16[4,32,512]{2,1,0:T(8,128)(2,1)S(1)} %pad_maximum_fusion.6), channel_id=1, source_target_pairs={{0,16},{4,20},{8,24},{12,28},{16,0},{20,4},{24,8},{28,12},{1,17},{... | collective-permute-start | bytes 393224 | tf_op jit(solution)/shard_map/ppermute | solution.py:21
  143.7 96.3 %reduce-scatter.11.cloned.1.call-start = ((), (), s32[]{:S(2)}) async-start(), calls=%async_computation.7 | async-start | bytes 1179648 | tf_op jit(solution)/shard_map/reduce_scatter | solution.py:117
  164.6 1.1 copy-start.13
  166.6 7.4 %copy-start.5 = (bf16[2,256,512]{2,1,0:T(8,128)(2,1)S(1)}, bf16[2,256,512]{2,1,0:T(8,128)(2,1)}, u32[]{:S(2)}) copy-start(bf16[2,256,512]{2,1,0:T(8,128)(2,1)} %param.26) | copy-start | bytes 1572868
  168.5 5.8 %copy-start.7 = (bf16[2,256,512]{2,1,0:T(8,128)(2,1)S(1)}, bf16[2,256,512]{2,1,0:T(8,128)(2,1)}, u32[]{:S(2)}) copy-start(bf16[2,256,512]{2,1,0:T(8,128)(2,1)} %param.25) | copy-start | bytes 1572868
  (7 other events, 5.7 us)
Sparse Core Ops, SparseCore 0:
  25.9 21.1 reduce-scatter.4
  60.3 64.2 reduce-scatter.6
  143.9 18.6 reduce-scatter.8
  175.8 64.1 reduce-scatter.10
